TPU v7x, 128 devices: a whole 4x4x4 slice. The times are simulated.
128 devices in a mesh: ep: 64 (over z, y, x), tp: 2 (over core).
Axes of the slice: x: 4, y: 4, z: 4, core: 2. Of those that a mesh axis runs over, the one named last changes fastest.
Arguments:
- tokens: bfloat16 [12288, 2048], P('ep', 'tp'), may hold values from -6 to 6
- chosen: int32 [64, 1536], P('ep'), may hold values from 0 to 12287, as said below
- gate_score: float32 [64, 1536], P('ep'), may hold values from 0.1 to 1
- gate_weight: bfloat16 [64, 2048, 2048], P('ep', None, 'tp'), may hold values from -0.125 to 0.125
- up_weight: bfloat16 [64, 2048, 2048], P('ep', None, 'tp'), may hold values from -0.125 to 0.125
- down_weight: bfloat16 [64, 2048, 2048], P('ep', 'tp'), may hold values from -0.125 to 0.125
Outputs:
- mixed: bfloat16 [12288, 2048], P('ep', 'tp')
Inputs may be any that keep to these rules, and one draw needn't show every extreme that they name: For every expert and every s, columns s * 24 to (s + 1) * 24 - 1 of chosen name 24 different tokens, all among tokens s * 192 to (s + 1) * 192 - 1.
All inputs are finite; a program needn't handle non-finite values.
Results may differ from a plain program's by a relative error of at most 0.012.
Values may be sent and summed in bfloat16 or wider, within the bound.
A program may use at most 128 MiB of HBM per device.

v0:
```python
import jax
import jax.numpy as jnp
from jax import lax
from jax.sharding import PartitionSpec as P


def in_order(blocks, dim):
    dims = list(blocks.shape[1:])
    dims[dim] *= blocks.shape[0]
    return jnp.moveaxis(blocks, 0, dim).reshape(dims)


def sent_to_all(array, axis):
    copies = jnp.broadcast_to(array, (lax.axis_size(axis), *array.shape))
    return lax.all_to_all(copies, axis, split_axis=0, concat_axis=0, tiled=True)


def gathered_copies(array, axis, dim):
    return in_order(sent_to_all(array, axis), dim)


def split_up(array, dim, length):
    dims = array.shape
    blocks = array.reshape(*dims[:dim], length, dims[dim] // length, *dims[dim + 1 :])
    return jnp.moveaxis(blocks, dim, 0)


def sum_at_owner(array, axis, dim):
    blocks = split_up(array, dim, lax.axis_size(axis))
    arrived = lax.all_to_all(blocks, axis, split_axis=0, concat_axis=0, tiled=True)
    return arrived.astype(jnp.float32).sum(axis=0)


def on_device(tokens, chosen, gate_score, gate_weight, up_weight, down_weight):
    ep_count = lax.axis_size("ep")
    tok_rows = tokens.shape[0]
    per_source = chosen.shape[1] // ep_count
    offset = lax.axis_index("ep") * tok_rows
    w_gate = gate_weight[0]
    w_up = up_weight[0]
    w_down = down_weight[0]
    owned_ids = lax.all_to_all(
        chosen.reshape(ep_count, per_source), "ep", split_axis=0, concat_axis=0, tiled=True
    )
    local_rows = owned_ids.reshape(-1) - offset
    outgoing = jnp.take(tokens, local_rows, axis=0).reshape(ep_count, per_source, -1)
    arrived = lax.all_to_all(outgoing, "ep", split_axis=0, concat_axis=0, tiled=True).reshape(
        ep_count * per_source, -1
    )
    shard_piece = gathered_copies(arrived, "tp", 1)
    gate_pre = jnp.dot(shard_piece, w_gate, preferred_element_type=jnp.float32)
    up_pre = jnp.dot(shard_piece, w_up, preferred_element_type=jnp.float32)
    hidden = (jax.nn.silu(gate_pre) * up_pre).astype(jnp.bfloat16)
    summed = sum_at_owner(
        jnp.einsum("fd,cf->dc", w_down, hidden, preferred_element_type=jnp.float32).astype(
            jnp.bfloat16
        ),
        "tp",
        0,
    )
    weighted = (summed * gate_score[0][None, :]).astype(jnp.bfloat16)
    returned = lax.all_to_all(weighted, "ep", split_axis=1, concat_axis=1, tiled=True)
    positions = lax.broadcasted_iota(jnp.int32, (tok_rows, 1), 0)
    selector = (positions == local_rows[None, :]).astype(jnp.bfloat16)
    mixed_out = jnp.einsum("tc,dc->td", selector, returned, preferred_element_type=jnp.float32)
    return mixed_out.astype(jnp.bfloat16)


def solution(mesh):
    in_specs = (
        P("ep", "tp"),
        P("ep", None),
        P("ep", None),
        P("ep", None, "tp"),
        P("ep", None, "tp"),
        P("ep", "tp", None),
    )
    out_specs = P("ep", "tp")
    return jax.shard_map(
        on_device, mesh=mesh, in_specs=in_specs, out_specs=out_specs, check_vma=False
    )
```

profile of v0, /device:TPU:1, one launch (start us, length us, event | category | flops | bytes accessed | tf_op | source)
XLA Modules:
  0.0 189.1 jit_solution(4841234242044043721)
XLA Ops:
  0.0 0.0 copy-start
  0.0 0.8 reduce
  0.8 0.7 all_to_all.21
  1.5 12.0 %all-to-all-start = ((s32[64,1,24]{2,1,0:T(1,128)}), s32[64,1,24]{2,1,0:T(1,128)S(1)}, u32[]{:S(2)}, u32[]{:S(2)}) async-start(s32[64,1,24]{2,1,0:T(1,128)} %bitcast), calls=%async_computation | async-start | bytes 65536 | tf_op jit(solution)/shard_map/all_to_all | solution.py:42
  13.4 8.3 %all-to-all-done = s32[64,1,24]{2,1,0:T(1,128)S(1)} async-done(((s32[64,1,24]{2,1,0:T(1,128)}), s32[64,1,24]{2,1,0:T(1,128)S(1)}, u32[]{:S(2)}, u32[]{:S(2)}) %all-to-all-start) | async-done | bytes 6176 | tf_op jit(solution)/shard_map/all_to_all | solution.py:42
  21.8 0.6 broadcast.67
  22.4 1.4 fusion.10
  23.8 0.1 sub.33
  23.9 0.0 copy-done
  23.9 5.1 %gather_fusion = bf16[1536,1024]{1,0:T(8,128)(2,1)S(1)} fusion(bf16[192,1024]{1,0:T(8,128)(2,1)S(1)} %copy-done, s32[2048]{0:T(1024)S(1)} %pad_clamp_fusion), kind=kCustom, calls=%fused_computation | custom fusion | bytes 6297600 | tf_op jit(solution)/shard_map/jit(_take)/gather | solution.py:46
  29.0 1.9 %broadcast_select_fusion = bf16[64,24,1024]{2,1,0:T(8,128)(2,1)} fusion(bf16[64,24,1024]{2,1,0:T(8,128)(2,1)S(1)} %bitcast.32, pred[64,24]{1,0:T(8,128)(4,1)S(1)} %compare_and_fusion), kind=kLoop, calls=%fused_computation.11 | loop fusion | flops 1572864 | bytes 6292992 | tf_op jit(solution)/shard_map/jit(_take)/select_n | solution.py:46
  30.9 0.0 copy-start.4
  30.9 4.9 %all-to-all-start.1 = ((bf16[64,24,1024]{2,1,0:T(8,128)(2,1)}), bf16[64,24,1024]{2,1,0:T(8,128)(2,1)S(1)}, u32[]{:S(2)}, u32[]{:S(2)}) async-start(bf16[64,24,1024]{2,1,0:T(8,128)(2,1)} %broadcast_select_fusion), calls=%async_computation.1 | async-start | bytes 6291456 | tf_op jit(solution)/shard_map/all_to_all | solution.py:47
  35.8 0.0 copy-done.4
  35.9 0.7 mul.24
  36.5 38.1 %all-to-all-done.1 = bf16[64,24,1024]{2,1,0:T(8,128)(2,1)S(1)} async-done(((bf16[64,24,1024]{2,1,0:T(8,128)(2,1)}), bf16[64,24,1024]{2,1,0:T(8,128)(2,1)S(1)}, u32[]{:S(2)}, u32[]{:S(2)}) %all-to-all-start.1) | async-done | bytes 3145760 | tf_op jit(solution)/shard_map/all_to_all | solution.py:47
  74.7 3.0 %copy.9 = bf16[1536,1024]{0,1:T(8,128)(2,1)} copy(bf16[1536,1024]{1,0:T(8,128)(2,1)S(1)} %bitcast.31) | data formatting | bytes 6291456 | tf_op jit(solution)/shard_map/reshape | solution.py:47
  77.6 2.3 %broadcast_in_dim.16 = bf16[2,1536,1024]{1,2,0:T(8,128)(2,1)S(1)} broadcast(bf16[1536,1024]{0,1:T(8,128)(2,1)} %copy.9), dimensions={1,2} | broadcast | bytes 9437184 | tf_op jit(solution)/shard_map/broadcast_in_dim | solution.py:14
  79.9 0.0 copy-start.5
  79.9 12.5 %all_to_all.33 = bf16[2,1536,1024]{1,2,0:T(8,128)(2,1)S(1)} all-to-all(bf16[2,1536,1024]{1,2,0:T(8,128)(2,1)S(1)} %broadcast_in_dim.16), channel_id=1, replica_groups=mesh['ep'=64,'tp'=2] {'tp'}, dimensions={0} | all-to-all | bytes 12582912 | tf_op jit(solution)/shard_map/all_to_all | solution.py:15
  92.4 0.0 copy-start.2
  92.4 2.7 %copy-done.2 = bf16[2,1536,1024]{1,2,0:T(8,128)(2,1)} copy-done((bf16[2,1536,1024]{1,2,0:T(8,128)(2,1)}, bf16[2,1536,1024]{1,2,0:T(8,128)(2,1)S(1)}, u32[]{:S(2)}) %copy-start.2) | copy-done | bytes 6291480
  95.1 0.0 copy-done.5
  95.1 8.8 %fusion.4 = f32[1536,1024]{1,0:T(8,128)} fusion(bf16[1536,2048]{0,1:T(8,128)(2,1)S(1)} %bitcast.33, bf16[1,2048,1024]{2,1,0:T(8,128)(2,1)S(1)} %copy-done.5), kind=kOutput, calls=%fused_computation.8 | convolution fusion | flops 6442450944 | bytes 16777216 | tf_op jit(solution)/shard_map/dot_general | solution.py:51
  103.9 21.1 %convolution_convert_fusion = bf16[1536,2048]{1,0:T(8,128)(2,1)} fusion(bf16[1,1024,2048]{2,1,0:T(8,128)(2,1)} %param.11, f32[1536,1024]{1,0:T(8,128)} %fusion.4, bf16[1536,2048]{0,1:T(8,128)(2,1)} %bitcast.34, bf16[1,2048,1024]{2,1,0:T(8,128)(2,1)} %param.10), kind=kOutput, calls=%fused_computation.2 | convolution fusion | flops 12897484800 | bytes 27262976 | tf_op jit(solution)/shard_map/fd,cf->dc/dot_general | solution.py:55
  125.0 3.5 %copy.13 = bf16[192,2,8,1024]{3,2,0,1:T(8,128)(2,1)S(1)} copy(bf16[192,2,8,1024]{3,2,1,0:T(8,128)(2,1)} %bitcast.35) | data formatting | bytes 12582912 | tf_op jit(solution)/shard_map/reshape | solution.py:24
  128.5 8.7 %all_to_all.34 = bf16[2,1024,1536]{1,2,0:T(8,128)(2,1)S(1)} all-to-all(bf16[2,1024,1536]{1,2,0:T(8,128)(2,1)S(1)} %bitcast.30), channel_id=1, replica_groups=mesh['ep'=64,'tp'=2] {'tp'}, dimensions={0} | all-to-all | bytes 12582912 | tf_op jit(solution)/shard_map/all_to_all | solution.py:30
  137.2 0.0 copy-start.3
  137.2 1.7 convert_reduce_fusion
  138.9 0.0 copy-done.3
  138.9 0.0 copy-start.1
  138.9 2.1 %multiply_convert_fusion = bf16[1024,64,24]{0,2,1:T(8,128)(2,1)} fusion(f32[1024,64,24]{0,2,1:T(8,128)S(1)} %bitcast.29, f32[64,24]{1,0:T(8,128)S(1)} %copy-done.3), kind=kLoop, calls=%fused_computation.4 | loop fusion | flops 3145728 | bytes 9443328 | tf_op jit(solution)/shard_map/convert_element_type | solution.py:61
  141.0 6.7 %all-to-all-start.4 = ((bf16[1024,64,24]{0,2,1:T(8,128)(2,1)}), bf16[1024,64,24]{0,2,1:T(8,128)(2,1)S(1)}, u32[]{:S(2)}, u32[]{:S(2)}) async-start(bf16[1024,64,24]{0,2,1:T(8,128)(2,1)} %multiply_convert_fusion), calls=%async_computation.4 | async-start | bytes 6291456 | tf_op jit(solution)/shard_map/all_to_all | solution.py:62
  147.7 0.8 sub.31
  148.5 39.1 %all-to-all-done.4 = bf16[1024,64,24]{0,2,1:T(8,128)(2,1)S(1)} async-done(((bf16[1024,64,24]{0,2,1:T(8,128)(2,1)}), bf16[1024,64,24]{0,2,1:T(8,128)(2,1)S(1)}, u32[]{:S(2)}, u32[]{:S(2)}) %all-to-all-start.4) | async-done | bytes 3145760 | tf_op jit(solution)/shard_map/all_to_all | solution.py:62
  187.6 1.5 convolution_convert_fusion.1
  189.1 0.0 copy-done.1
  (4 shorter events, 0.1 us)
Async XLA Ops:
  0.0 23.9 %copy-start = (bf16[192,1024]{1,0:T(8,128)(2,1)S(1)}, bf16[192,1024]{1,0:T(8,128)(2,1)}, u32[]{:S(2)}) copy-start(bf16[192,1024]{1,0:T(8,128)(2,1)} %param.6) | copy-start | bytes 1179652
  1.5 20.3 %all-to-all-start = ((s32[64,1,24]{2,1,0:T(1,128)}), s32[64,1,24]{2,1,0:T(1,128)S(1)}, u32[]{:S(2)}, u32[]{:S(2)}) async-start(s32[64,1,24]{2,1,0:T(1,128)} %bitcast), calls=%async_computation | async-start | bytes 65536 | tf_op jit(solution)/shard_map/all_to_all | solution.py:42
  30.9 4.9 %copy-start.4 = (f32[1,1536]{1,0:T(1,128)S(1)}, f32[1,1536]{1,0:T(1,128)}, u32[]{:S(2)}) copy-start(f32[1,1536]{1,0:T(1,128)} %param.8) | copy-start | bytes 18436
  30.9 43.7 %all-to-all-start.1 = ((bf16[64,24,1024]{2,1,0:T(8,128)(2,1)}), bf16[64,24,1024]{2,1,0:T(8,128)(2,1)S(1)}, u32[]{:S(2)}, u32[]{:S(2)}) async-start(bf16[64,24,1024]{2,1,0:T(8,128)(2,1)} %broadcast_select_fusion), calls=%async_computation.1 | async-start | bytes 6291456 | tf_op jit(solution)/shard_map/all_to_all | solution.py:47
  79.9 15.2 %copy-start.5 = (bf16[1,2048,1024]{2,1,0:T(8,128)(2,1)S(1)}, bf16[1,2048,1024]{2,1,0:T(8,128)(2,1)}, u32[]{:S(2)}) copy-start(bf16[1,2048,1024]{2,1,0:T(8,128)(2,1)} %param.9) | copy-start | bytes 12582916
  92.4 2.7 %copy-start.2 = (bf16[2,1536,1024]{1,2,0:T(8,128)(2,1)}, bf16[2,1536,1024]{1,2,0:T(8,128)(2,1)S(1)}, u32[]{:S(2)}) copy-start(bf16[2,1536,1024]{1,2,0:T(8,128)(2,1)S(1)} %all_to_all.33) | copy-start | bytes 18874372
  137.2 1.7 copy-start.3
  138.9 50.2 %copy-start.1 = (bf16[192,1024]{1,0:T(8,128)(2,1)S(1)}, bf16[192,1024]{1,0:T(8,128)(2,1)}, u32[]{:S(2)}) copy-start(bf16[192,1024]{1,0:T(8,128)(2,1)} %param.6) | copy-start | bytes 1179652
  141.0 46.6 %all-to-all-start.4 = ((bf16[1024,64,24]{0,2,1:T(8,128)(2,1)}), bf16[1024,64,24]{0,2,1:T(8,128)(2,1)S(1)}, u32[]{:S(2)}, u32[]{:S(2)}) async-start(bf16[1024,64,24]{0,2,1:T(8,128)(2,1)} %multiply_convert_fusion), calls=%async_computation.4 | async-start | bytes 6291456 | tf_op jit(solution)/shard_map/all_to_all | solution.py:62
where the time goes:
time: 191 us; the launch traced here: 189 us
  waiting for transfers between devices  85.5 us (45%)
  matrix products  31.4 us (16%)
  starting transfers between devices  23.5 us (12%)
  blocking collectives  21.2 us (11%)
  local copies, waits for them, and re-layouts  19.4 us (10%)
  other arithmetic  7.92 us (4%)
    all_to_all x1, waiting for transfers between devices, on_device(): lax.all_to_all(weighted, 'ep', split_axis=1, concat_axis=1, tiled=True)  39.1 us
    all_to_all x1, waiting for transfers between devices, on_device(): lax.all_to_all(outgoing, 'ep', split_axis=0, concat_axis=0, tiled=True)  38.1 us
    dot_general x1, matrix products, on_device(): jnp.einsum('fd,cf->dc', w_down, hidden, preferred_element_type=jnp.float32)  21.1 us
    all_to_all x1, blocking collectives, sent_to_all(): return lax.all_to_all(copies, axis, split_axis=0, concat_axis=0, tiled=True)  12.5 us
    all_to_all x1, starting transfers between devices, on_device(): lax.all_to_all(chosen.reshape(ep_count, per_source), 'ep', split_axis=0,...  12 us
    dot_general x1, matrix products, on_device(): gate_pre = jnp.dot(shard_piece, w_gate, preferred_element_type=jnp.float32)  8.77 us
    all_to_all x1, blocking collectives, sum_at_owner(): lax.all_to_all(blocks, axis, split_axis=0, concat_axis=0, tiled=True)  8.71 us
    all_to_all x1, waiting for transfers between devices, on_device(): lax.all_to_all(chosen.reshape(ep_count, per_source), 'ep', split_axis=0,...  8.35 us
  transfers between devices with their start and end apart: 3, of which 3 were waited for; matrix products, arithmetic and copies ran while one was open for 1% of the time, Pallas kernels for 0%

commit v1 on v0

v1 whole, which is shorter than its diff:
```python
import jax
import jax.numpy as jnp
from jax import lax
from jax.experimental import pallas as pl
from jax.experimental.pallas import tpu as pltpu
from jax.sharding import PartitionSpec as P

BF16 = jnp.bfloat16
F32 = jnp.float32
MESH = pl.DeviceIdType.MESH
TOK = 192
PICK = 24
HALF = 1024
ROWS = 16 * PICK
SLICES = ((0, 384), (384, 384), (768, 256))


def offset_of(s, a, b, c):
    if s == 0:
        return c, a, b
    if s == 1:
        return a, c, b
    return a, b, c


def kernel(
    tokens, chosen, score, wg_hbm, wu_hbm, wd_hbm, out,
    wg, wu, wd, gathered, isend, irecv, pick, dsend, own, other, hidden, pown, psend, precv,
    wt, ret, sums, rsend, rrecv, scale,
    w_sem, i_send, i_recv, g_send, g_recv, d_send, d_recv, f_send, f_recv, p_send, p_recv,
    r_send, r_recv, q_send, q_recv,
):
    ep = lax.axis_index("ep")
    tp = lax.axis_index("tp")
    z, y, x = ep // 16, (ep // 4) % 4, ep % 4

    def peer(dz, dy, dx):
        return ((z + dz + 4) % 4) * 16 + ((y + dy + 4) % 4) * 4 + (x + dx + 4) % 4

    def remote(src, dst, send, recv, dev):
        return pltpu.make_async_remote_copy(
            src_ref=src, dst_ref=dst, send_sem=send, recv_sem=recv, device_id=dev, device_id_type=MESH
        )

    partner = (ep, 1 - tp)

    def block_of(s, a, b, c):
        dz, dy, dx = offset_of(s, a, b, c)
        return dy * 4 + dx

    weights = [
        pltpu.make_async_copy(src, dst, w_sem.at[i])
        for i, (src, dst) in enumerate(((wg_hbm, wg), (wu_hbm, wu), (wd_hbm, wd)))
    ]
    for copy in weights:
        copy.start()

    barrier = pltpu.get_barrier_semaphore()
    near = 0
    for dz in range(4):
        for dy in range(4):
            for dx in range(4):
                if (dz or dy or dx) and not (dz and dy and dx):
                    near += 1
                    pl.semaphore_signal(barrier, 1, device_id=(peer(dz, dy, dx), tp), device_id_type=MESH)
    pl.semaphore_signal(barrier, 1, device_id=partner, device_id_type=MESH)

    lane = lax.broadcasted_iota(jnp.int32, (64, 128), 1)
    local = chosen[...] - TOK * lax.broadcasted_iota(jnp.int32, (64, 128), 0) + 1
    local = jnp.where(lane < PICK, local, 0).astype(F32)
    shifted = jnp.concatenate(
        [local if a == 0 else pltpu.roll(local, a * PICK, 1) for a in range(4)], axis=0
    ).astype(BF16)
    row = lax.broadcasted_iota(jnp.int32, (128, 256), 0)
    col = lax.broadcasted_iota(jnp.int32, (128, 256), 1)
    ia, ib, ic = row >> 5, (row >> 3) & 3, row & 7
    for s in range(3):
        oz, oy, ox = offset_of(s, ia, ib, ic)
        src = ((z - oz) & 3) * 16 + ((y - oy) & 3) * 4 + ((x - ox) & 3)
        take = jnp.where((col == ia * 64 + src) & (ic < 4), 1.0, 0.0).astype(BF16)
        rows = jnp.dot(take, shifted, preferred_element_type=F32)
        isend[16 * s : 16 * s + 16] = rows.astype(BF16).reshape(16, 8, 128)
        irecv[16 * s] = rows[0:8].astype(BF16)
    gathered[0] = tokens[...]

    pl.semaphore_wait(barrier, near + 1)

    def send_rows(j, carry):
        a, b = j // 4, j % 4
        for s in range(3):
            remote(
                isend.at[16 * s + j], irecv.at[16 * s + j], i_send, i_recv,
                (peer(*offset_of(s, -a, -b, 0)), tp),
            ).start()
        return carry

    lax.fori_loop(1, 16, send_rows, 0)
    for c in (2, 1, 3):
        for s, (lo, width) in enumerate(SLICES):
            cols = pl.ds(lo, width)
            remote(
                tokens.at[:, cols], gathered.at[c, :, cols], g_send, g_recv,
                (peer(*offset_of(s, 0, 0, c)), tp),
            ).start()

    row = lax.broadcasted_iota(jnp.int32, (64, 64), 0)
    col = lax.broadcasted_iota(jnp.int32, (64, 64), 1)
    oy, ox = (row >> 2) & 3, row & 3
    oz = ((row >> 4) - oy - ox) & 3
    src = ((z - oz) & 3) * 16 + ((y - oy) & 3) * 4 + ((x - ox) & 3)
    ordered = jnp.dot(
        jnp.where(col == src, 1.0, 0.0), score[...], preferred_element_type=F32, precision=lax.Precision.HIGHEST
    )
    upright = ordered.T
    for o in range(64):
        scale[o * PICK : (o + 1) * PICK, :] = jnp.broadcast_to(upright[0:PICK, o : o + 1], (PICK, 128))

    remote(isend.at[0:45], irecv.at[0:45], i_send, i_recv, partner).wait_recv()
    token_row = lax.broadcasted_iota(jnp.int32, (TOK, 128), 0).astype(F32)

    def build(r, carry):
        for s in range(3):
            for c in range(4):
                total = jnp.zeros((8, 128), F32)
                for a in range(4):
                    b = (r - c - a + 8) % 4
                    total += irecv[16 * s + 4 * a + b].astype(F32)
                wanted = jnp.broadcast_to(total[c : c + 1] - 1.0, (TOK, 128))
                pick[(s * 4 + r) * 4 + c] = jnp.where(wanted == token_row, 1.0, 0.0).astype(BF16)
        return carry

    lax.fori_loop(0, 4, build, 0)
    remote(gathered.at[1:4], gathered.at[1:4], g_send, g_recv, partner).wait_recv()

    def dispatch(r, carry):
        for s, (lo, width) in enumerate(SLICES):
            for c in range(4):
                rows = lax.dot_general(
                    pick[(s * 4 + r) * 4 + c], gathered[c, :, lo : lo + width],
                    (((0,), (0,)), ((), ())), preferred_element_type=F32,
                ).astype(BF16)
                for a in range(4):
                    b = (r - c - a + 8) % 4
                    dsend[r * 16 + block_of(s, a, b, c), :, lo : lo + width] = rows[a * PICK : (a + 1) * PICK]
            mine = r * 16 + block_of(s, 0, 0, r)
            own[mine, :, lo : lo + width] = dsend[mine, :, lo : lo + width]

        def send(j, carry):
            a, b = j // 4, j % 4
            c = (r - a - b + 8) % 4
            for s, (lo, width) in enumerate(SLICES):
                blk = r * 16 + block_of(s, a, b, c)
                cols = pl.ds(lo, width)
                remote(
                    dsend.at[blk, :, cols], own.at[blk, :, cols], d_send, d_recv.at[r],
                    (peer(*offset_of(s, a, b, 0)), tp),
                ).start()
            return carry

        lax.fori_loop(1, 16, send, 0)
        return carry

    lax.fori_loop(0, 4, dispatch, 0)

    def forward(r):
        chunk = pl.ds(r * 16, 16)
        return remote(own.at[chunk], other.at[chunk], f_send, f_recv.at[r], partner)

    def pass_partial(r):
        return remote(psend.at[r], precv.at[r], p_send, p_recv.at[r], partner)

    def arrived(r):
        part = pl.ds(r * 16, 15)
        remote(own.at[part], own.at[part], d_send, d_recv.at[r], partner).wait_recv()

    def finish(r):
        pass_partial(r).wait_recv()
        factor = jnp.concatenate([scale[pl.ds(pl.multiple_of(r * ROWS, ROWS), ROWS), :]] * 2, axis=1)
        for n in range(4):
            cols = slice(n * 256, (n + 1) * 256)
            summed = pown[r, :, cols].astype(F32) + precv[r, :, cols].astype(F32)
            wt[pl.ds(r * 16, 16), :, cols] = (summed * factor).astype(BF16).reshape(16, PICK, 256)
        for s, (lo, width) in enumerate(SLICES):
            ret[r * 20, :, lo : lo + width] = wt[r * 16 + block_of(s, 0, 0, r), :, lo : lo + width]

        def send(j, carry):
            a, b = j // 4, j % 4
            c = (r - a - b + 8) % 4
            for s, (lo, width) in enumerate(SLICES):
                cols = pl.ds(lo, width)
                remote(
                    wt.at[r * 16 + block_of(s, a, b, c), :, cols], ret.at[r * 16 + c * 4 + a, :, cols],
                    r_send, r_recv.at[r], (peer(*offset_of(s, -a, -b, 0)), tp),
                ).start()
            return carry

        lax.fori_loop(1, 16, send, 0)

    for copy in weights:
        copy.wait()
    mine_at = pl.multiple_of(tp * HALF, HALF)
    other_at = pl.multiple_of((1 - tp) * HALF, HALF)

    def ffn(r, carry):
        arrived(r)
        forward(r).start()

        @pl.when(r > 0)
        def _():
            finish(r - 1)

        forward(r).wait_recv()
        x_own = own[pl.ds(r * 16, 16)].reshape(ROWS, HALF)
        x_other = other[pl.ds(r * 16, 16)].reshape(ROWS, HALF)
        for n in range(4):
            cols = slice(n * 256, (n + 1) * 256)
            gate = jnp.dot(x_own, wg[pl.ds(mine_at, HALF), cols], preferred_element_type=F32)
            gate += jnp.dot(x_other, wg[pl.ds(other_at, HALF), cols], preferred_element_type=F32)
            up = jnp.dot(x_own, wu[pl.ds(mine_at, HALF), cols], preferred_element_type=F32)
            up += jnp.dot(x_other, wu[pl.ds(other_at, HALF), cols], preferred_element_type=F32)
            hidden[:, cols] = (gate / (1.0 + jnp.exp(-gate)) * up).astype(BF16)
        for n in range(4):
            psend[r, :, n * 256 : (n + 1) * 256] = jnp.dot(
                hidden[...], wd[:, pl.ds(pl.multiple_of(other_at + n * 256, 256), 256)], preferred_element_type=F32
            ).astype(BF16)
        pass_partial(r).start()
        for n in range(4):
            pown[r, :, n * 256 : (n + 1) * 256] = jnp.dot(
                hidden[...], wd[:, pl.ds(pl.multiple_of(mine_at + n * 256, 256), 256)], preferred_element_type=F32
            ).astype(BF16)
        return carry

    lax.fori_loop(0, 4, ffn, 0)
    finish(3)

    sums[...] = jnp.zeros_like(sums)

    def combine(r, carry):
        part = pl.ds(r * 16, 15)
        remote(ret.at[part], ret.at[part], r_send, r_recv.at[r], partner).wait_recv()
        for s, (lo, width) in enumerate(SLICES):
            for c in range(4):
                rows = ret[pl.ds(r * 16 + c * 4, 4), :, lo : lo + width].reshape(4 * PICK, width)
                rows = jnp.concatenate([rows, jnp.zeros((128 - 4 * PICK, width), BF16)], axis=0)
                sums[c, :, lo : lo + width] += jnp.dot(
                    pick[(s * 4 + r) * 4 + c], rows, preferred_element_type=F32
                )
        return carry

    lax.fori_loop(0, 4, combine, 0)
    for c in (2, 1, 3):
        rsend[c - 1] = sums[c].astype(BF16)
        for s, (lo, width) in enumerate(SLICES):
            cols = pl.ds(lo, width)
            remote(
                rsend.at[c - 1, :, cols], rrecv.at[c - 1, :, cols], q_send, q_recv,
                (peer(*offset_of(s, 0, 0, -c)), tp),
            ).start()
    remote(rrecv.at[0:3], rrecv.at[0:3], q_send, q_recv, partner).wait_recv()
    total = sums[0]
    for c in range(3):
        total += rrecv[c].astype(F32)
    out[...] = total.astype(BF16)

    remote(isend.at[0:45], irecv.at[0:45], i_send, i_recv, partner).wait_send()
    remote(gathered.at[1:4], gathered.at[1:4], g_send, g_recv, partner).wait_send()
    remote(dsend.at[0:60], dsend.at[0:60], d_send, d_recv.at[0], partner).wait_send()
    remote(own, other, f_send, f_recv.at[0], partner).wait_send()
    remote(psend, precv, p_send, p_recv.at[0], partner).wait_send()
    remote(wt.at[0:60], ret.at[0:60], r_send, r_recv.at[0], partner).wait_send()
    remote(rsend, rrecv, q_send, q_recv, partner).wait_send()


def on_device(tokens, chosen, gate_score, gate_weight, up_weight, down_weight):
    vmem = pl.BlockSpec(memory_space=pltpu.VMEM)
    hbm = pl.BlockSpec(memory_space=pl.ANY)
    dma = pltpu.SemaphoreType.DMA
    chosen = jnp.pad(chosen.reshape(64, PICK), ((0, 0), (0, 128 - PICK)))
    score = jnp.pad(gate_score.reshape(64, PICK), ((0, 0), (0, 128 - PICK)))
    blocks = pltpu.VMEM((64, PICK, HALF), BF16)
    partial = pltpu.VMEM((4, ROWS, HALF), BF16)
    return pl.pallas_call(
        kernel,
        out_shape=jax.ShapeDtypeStruct((TOK, HALF), BF16),
        in_specs=[vmem, vmem, vmem, hbm, hbm, hbm],
        out_specs=vmem,
        scratch_shapes=[
            pltpu.VMEM((2048, 1024), BF16), pltpu.VMEM((2048, 1024), BF16), pltpu.VMEM((1024, 2048), BF16),
            pltpu.VMEM((4, TOK, HALF), BF16),
            pltpu.VMEM((48, 8, 128), BF16), pltpu.VMEM((48, 8, 128), BF16),
            pltpu.VMEM((48, TOK, 128), BF16),
            blocks, blocks, blocks,
            pltpu.VMEM((ROWS, 1024), BF16),
            partial, partial, partial,
            blocks, blocks,
            pltpu.VMEM((4, TOK, HALF), F32),
            pltpu.VMEM((3, TOK, HALF), BF16), pltpu.VMEM((3, TOK, HALF), BF16),
            pltpu.VMEM((64 * PICK, 128), F32),
            dma((3,)), dma, dma, dma, dma, dma, dma((4,)), dma, dma((4,)), dma, dma((4,)),
            dma, dma((4,)), dma, dma,
        ],
        compiler_params=pltpu.CompilerParams(
            collective_id=0, has_side_effects=True, vmem_limit_bytes=63 << 20
        ),
        cost_estimate=pl.CostEstimate(flops=20_000_000_000, bytes_accessed=14_000_000, transcendentals=1_600_000),
    )(tokens, chosen, score, gate_weight[0], up_weight[0], down_weight[0])


def solution(mesh):
    in_specs = (
        P("ep", "tp"),
        P("ep", None),
        P("ep", None),
        P("ep", None, "tp"),
        P("ep", None, "tp"),
        P("ep", "tp", None),
    )
    out_specs = P("ep", "tp")
    return jax.shard_map(
        on_device, mesh=mesh, in_specs=in_specs, out_specs=out_specs, check_vma=False
    )
```

time: 191 us -> 87.8 us (0.46)
  waiting for transfers between devices: 85.5 us -> 0 us
  Pallas kernels: 0 us -> 82.9 us
  matrix products: 31.4 us -> 0 us
  starting transfers between devices: 23.5 us -> 0 us
  blocking collectives: 21.2 us -> 0 us
  local copies, waits for them, and re-layouts: 19.4 us -> 3.16 us
  other arithmetic: 7.92 us -> 1.43 us
    all_to_all x3 -> x0, waiting for transfers between devices: 85.5 us -> none  [the longest x1 39.1 us: on_device(): lax.all_to_all(weighted, 'ep', split_axis=1, concat_axis=1, tiled=True)]
    pallas_call x0 -> x1, Pallas kernels: none -> 82.9 us  [on_device(): pl.pallas_call(kernel, out_shape=jax.ShapeDtypeStruct((TOK, HALF), BF16),...]
    dot_general x3 -> x0, matrix products: 31.4 us -> none  [the longest x1 21.1 us: on_device(): jnp.einsum('fd,cf->dc', w_down, hidden, preferred_element_type=jnp.float32)]
    all_to_all x3 -> x0, starting transfers between devices: 23.5 us -> none  [the longest x1 12 us: on_device(): lax.all_to_all(chosen.reshape(ep_count, per_source), 'ep', split_axis=0,...]
    all_to_all x2 -> x0, blocking collectives: 21.2 us -> none  [the longest x1 12.5 us: sent_to_all(): return lax.all_to_all(copies, axis, split_axis=0, concat_axis=0, tiled=True)]
    reshape x2, local copies, waits for them, and re-layouts: 6.45 us -> 0.16 us  [the longest x1 0.08 us: on_device(): score = jnp.pad(gate_score.reshape(64, PICK), ((0, 0), (0, 128 - PICK)))]
    gather x1 -> x0, local copies, waits for them, and re-layouts: 5.07 us -> none  [on_device(): jnp.take(tokens, local_rows, axis=0).reshape(ep_count, per_source, -1)]
    broadcast_in_dim x1 -> x0, local copies, waits for them, and re-layouts: 2.3 us -> none  [sent_to_all(): copies = jnp.broadcast_to(array, (lax.axis_size(axis), *array.shape))]
  transfers between devices with their start and end apart: 3 -> 0, of which waited for: 3 -> 0; matrix products, arithmetic and copies ran while one was open for 1% -> 0% of each run, Pallas kernels for 0% -> 0%
where the time goes in v1:
time: 87.8 us; the launch traced here: 87.5 us
  Pallas kernels  82.9 us (94%)
  local copies, waits for them, and re-layouts  3.16 us (4%)
  other arithmetic  1.43 us (2%)
    pallas_call x1, Pallas kernels, on_device(): pl.pallas_call(kernel, out_shape=jax.ShapeDtypeStruct((TOK, HALF), BF16),...  82.9 us
    unnamed x1, local copies, waits for them, and re-layouts  1.77 us

profile of v1, /device:TPU:1, one launch (start us, length us, event | category | flops | bytes accessed | tf_op | source)
XLA Modules:
  0.0 87.5 jit_solution(12515138694013908722)
XLA Ops:
  0.0 0.7 reduce
  0.7 0.7 reduce.1
  1.4 0.1 reshape.7
  1.5 0.6 pad.9.score
  2.1 0.1 reshape.6
  2.2 0.6 pad.8.chosen
  2.8 82.9 %shard_map.64 = bf16[192,1024]{1,0:T(8,128)(2,1)} custom-call(bf16[192,1024]{1,0:T(8,128)(2,1)} %tokens.1, s32[64,128]{1,0:T(8,128)} %pad.8.chosen, f32[64,128]{1,0:T(8,128)} %pad.9.score, bf16[2048,1024]{1,0:T(8,128)(2,1)} %bitcast.3, bf16[2048,1024]{1,0:T(8,128)(2,1)} %bitcast.4, bf16[1024,2048]{1,0:T(8,128)(2,1)} %bitcast.5), custom_call_target="tpu_custom_call" | custom-call | flops 20000000000 | bytes 14000000 | tf_op jit(solution)/shard_map/pallas_call | solution.py:282
  85.8 1.8 %copy.8 = bf16[192,1024]{1,0:T(8,128)(2,1)} copy(bf16[192,1024]{1,0:T(8,128)(2,1)} %shard_map.64) | data formatting | bytes 786432

commit v2 on v1

v2 whole, which is shorter than its diff:
```python
import jax
import jax.numpy as jnp
from jax import lax
from jax.experimental import pallas as pl
from jax.experimental.pallas import tpu as pltpu
from jax.sharding import PartitionSpec as P

BF16 = jnp.bfloat16
F32 = jnp.float32
MESH = pl.DeviceIdType.MESH
TOK = 192
PICK = 24
HALF = 1024
ROWS = 16 * PICK
CAP = 64 * PICK
SLICES = ((0, 384), (384, 384), (768, 256))


def offset_of(s, a, b, c):
    if s == 0:
        return c, a, b
    if s == 1:
        return a, c, b
    return a, b, c


def kernel(
    tokens, chosen, score, wg_hbm, wu_hbm, wd_hbm, out,
    wg, wu, wd, gathered, isend, passed, irecv, pick, dsend, own, other, gate_acc, up_acc, hidden, pown, psend, precv,
    wt, ret, sums, rsend, rrecv, scale,
    w_sem, i_send, i_recv, j_send, j_recv, g_send, g_recv, d_send, d_recv, f_send, f_recv, p_send, p_recv,
    r_send, r_recv, q_send, q_recv,
):
    ep = lax.axis_index("ep")
    tp = lax.axis_index("tp")
    z, y, x = ep // 16, (ep // 4) % 4, ep % 4
    u, v = y + tp * (x - y), x + tp * (y - x)
    u_step, v_step = 4 - 3 * tp, 1 + 3 * tp

    z_at = [lax.rem(z + k, 4) * 16 for k in range(4)]
    u_at = [lax.rem(u + k, 4) * u_step for k in range(4)]
    v_at = [lax.rem(v + k, 4) * v_step for k in range(4)]

    def peer(dz, du, dv):
        return z_at[dz % 4] + u_at[du % 4] + v_at[dv % 4]

    def remote(src, dst, send, recv, dev):
        return pltpu.make_async_remote_copy(
            src_ref=src, dst_ref=dst, send_sem=send, recv_sem=recv, device_id=dev, device_id_type=MESH
        )

    partner = (ep, 1 - tp)

    def block_of(s, a, b, c):
        dz, du, dv = offset_of(s, a, b, c)
        return du * u_step + dv * v_step

    weights = [
        pltpu.make_async_copy(src, dst, w_sem.at[i])
        for i, (src, dst) in enumerate(((wg_hbm, wg), (wu_hbm, wu), (wd_hbm, wd)))
    ]
    for copy in weights:
        copy.start()

    barrier = pltpu.get_barrier_semaphore()
    for s in range(3):
        for c in (2, 1, 3):
            pl.semaphore_signal(
                barrier, 1, device_id=(peer(*offset_of(s, 0, 0, c)), tp), device_id_type=MESH
            )
    pl.semaphore_signal(barrier, 1, device_id=partner, device_id_type=MESH)

    lane = lax.broadcasted_iota(jnp.int32, (1, CAP), 1)
    home = ((lane.astype(F32) + 0.5) * (1.0 / PICK)).astype(jnp.int32)
    local = (chosen[...] - TOK * home + 1).astype(F32)
    place = lax.broadcasted_iota(jnp.int32, (CAP, 128), 0)
    place -= PICK * ((place.astype(F32) + 0.5) * (1.0 / PICK)).astype(jnp.int32)
    place = lax.broadcasted_iota(jnp.int32, (CAP, 128), 1) - place
    row = lax.broadcasted_iota(jnp.int32, (32, CAP), 0)
    ib, ic = row >> 3, row & 7
    homes = jnp.broadcast_to(home, (32, CAP))
    locals_ = jnp.broadcast_to(local, (32, CAP))
    for a in range(4):
        spread = jnp.where(place == a * PICK, 1.0, 0.0).astype(BF16)
        for s in range(3):
            oz, ou, ov = offset_of(s, a, ib, ic)
            src = ((z - oz) & 3) * 16 + ((u - ou) & 3) * u_step + ((v - ov) & 3) * v_step
            src = jnp.where(ic < 4, src, -1)
            take = jnp.where(homes == src, locals_, 0.0).astype(BF16)
            rows = jnp.dot(take, spread, preferred_element_type=F32).astype(BF16)
            isend[s, a] = rows.reshape(4, 8, 128)
            if a == 0:
                passed[s, :, 0] = rows.reshape(4, 8, 128)
    gathered[0] = tokens[...]

    pl.semaphore_wait(barrier, 10)

    for s in range(3):
        for a in (2, 1, 3):
            remote(
                isend.at[s, a], passed.at[s, :, a], i_send, i_recv, (peer(*offset_of(s, -a, 0, 0)), tp)
            ).start()

    def gather(c, lines):
        for s, (lo, width) in enumerate(SLICES):
            cols = pl.ds(lo, width)
            remote(
                tokens.at[lines, cols], gathered.at[c, lines, cols], g_send, g_recv,
                (peer(*offset_of(s, 0, 0, c)), tp),
            ).start()

    gather(1, pl.ds(0, 128))
    gather(3, pl.ds(0, 128))
    remote(passed.at[:, :, 0:3], passed.at[:, :, 1:4], i_send, i_recv, partner).wait_recv()
    for s in range(3):
        for b in (2, 1, 3):
            remote(
                passed.at[s, b], irecv.at[s, b], j_send, j_recv, (peer(*offset_of(s, 0, -b, 0)), tp)
            ).start()
        irecv[s, 0] = passed[s, 0]
    gather(1, pl.ds(128, 64))
    gather(3, pl.ds(128, 64))
    gather(2, pl.ds(0, TOK))

    row = lax.broadcasted_iota(jnp.int32, (64, CAP), 0)
    oy, ox = (row >> 2) & 3, row & 3
    oz = ((row >> 4) - oy - ox) & 3
    src = ((z - oz) & 3) * 16 + ((y - oy) & 3) * 4 + ((x - ox) & 3)
    left = jnp.where(jnp.broadcast_to(home, (64, CAP)) == src, jnp.broadcast_to(score[...], (64, CAP)), 0.0)
    spread = jnp.where(place == 0, 1.0, 0.0).astype(BF16)
    ordered = jnp.zeros((64, 128), F32)
    for _ in range(3):
        term = left.astype(BF16)
        ordered += jnp.dot(term, spread, preferred_element_type=F32)
        left -= term.astype(F32)
    upright = ordered.T
    for o in range(64):
        scale[o * PICK : (o + 1) * PICK, :] = jnp.broadcast_to(upright[0:PICK, o : o + 1], (PICK, 128))

    remote(irecv.at[:, 0:3], irecv.at[:, 1:4], j_send, j_recv, partner).wait_recv()
    token_row = lax.broadcasted_iota(jnp.int32, (TOK, 128), 0).astype(F32)

    def dispatch(r, c):
        for s, (lo, width) in enumerate(SLICES):
            cols = pl.ds(lo, width)
            total = irecv[s, (r - c) % 4, 0].astype(F32)
            for a in range(1, 4):
                total += irecv[s, (r - c - a) % 4, a].astype(F32)
            wanted = jnp.broadcast_to(total[c : c + 1] - 1.0, (TOK, 128))
            chosen_rows = jnp.where(wanted == token_row, 1.0, 0.0).astype(BF16)
            pick[(s * 4 + r) * 4 + c] = chosen_rows
            rows = lax.dot_general(
                chosen_rows, gathered[c, :, lo : lo + width],
                (((0,), (0,)), ((), ())), preferred_element_type=F32,
            ).astype(BF16)
            for a in range(4):
                b = (r - c - a) % 4
                blk = r * 16 + block_of(s, a, b, c)
                if a == 0 and b == 0:
                    own[blk, :, lo : lo + width] = rows[0:PICK]
                    continue
                dsend[blk, :, lo : lo + width] = rows[a * PICK : (a + 1) * PICK]
                remote(
                    dsend.at[blk, :, cols], own.at[blk, :, cols], d_send, d_recv.at[r],
                    (peer(*offset_of(s, a, b, 0)), tp),
                ).start()

    dispatch(0, 0)
    dispatch(1, 0)
    remote(gathered.at[0:3], gathered.at[1:4], g_send, g_recv, partner).wait_recv()
    for r in range(4):
        for c in (0, 1, 3, 2):
            if c or r > 1:
                dispatch(r, c)

    def forward(r):
        chunk = pl.ds(r * 16, 16)
        return remote(own.at[chunk], other.at[chunk], f_send, f_recv.at[r], partner)

    def pass_partial(r, half):
        return remote(psend.at[r, half], precv.at[r, half], p_send, p_recv.at[r, half], partner)

    def arrived(r):
        part = pl.ds(r * 16, 15)
        remote(own.at[part], own.at[part], d_send, d_recv.at[r], partner).wait_recv()

    def finish(r):
        back = [lax.rem(r + 4 - k, 4) for k in range(4)]
        first = pl.multiple_of(r * ROWS, ROWS)
        factor = jnp.concatenate([scale[pl.ds(first, ROWS), :]] * 4, axis=1)
        for half in range(2):
            pass_partial(r, half).wait_recv()
            summed = pown[r, half].astype(F32) + precv[r, half].astype(F32)
            wt[pl.ds(r * 16, 16), :, half * 512 : half * 512 + 512] = (
                (summed * factor).astype(BF16).reshape(16, PICK, 512)
            )
            for s, (lo, width) in enumerate(SLICES):
                if (lo + width > 512) != (half == 1):
                    continue
                cols = pl.ds(lo, width)
                ret[r * 20, :, lo : lo + width] = wt[r * 16 + block_of(s, 0, 0, r), :, lo : lo + width]
                for j in range(1, 16):
                    a, b = j // 4, j % 4
                    c = back[(a + b) % 4]
                    remote(
                        wt.at[r * 16 + block_of(s, a, b, c), :, cols], ret.at[r * 16 + c * 4 + a, :, cols],
                        r_send, r_recv.at[r, s], (peer(*offset_of(s, -a, -b, 0)), tp),
                    ).start()

    for copy in weights:
        copy.wait()
    mine_at = pl.multiple_of(tp * HALF, HALF)
    other_at = pl.multiple_of((1 - tp) * HALF, HALF)

    def ffn(r, carry):
        arrived(r)
        forward(r).start()
        x_own = own[pl.ds(r * 16, 16)].reshape(ROWS, HALF)
        for n in range(4):
            cols = slice(n * 256, (n + 1) * 256)
            gate_acc[:, cols] = jnp.dot(x_own, wg[pl.ds(mine_at, HALF), cols], preferred_element_type=F32)

        @pl.when(r > 0)
        def _():
            finish(r - 1)

        for n in range(4):
            cols = slice(n * 256, (n + 1) * 256)
            up_acc[:, cols] = jnp.dot(x_own, wu[pl.ds(mine_at, HALF), cols], preferred_element_type=F32)
        forward(r).wait_recv()
        x_other = other[pl.ds(r * 16, 16)].reshape(ROWS, HALF)
        for n in range(4):
            cols = slice(n * 256, (n + 1) * 256)
            gate = gate_acc[:, cols] + jnp.dot(
                x_other, wg[pl.ds(other_at, HALF), cols], preferred_element_type=F32
            )
            up = up_acc[:, cols] + jnp.dot(x_other, wu[pl.ds(other_at, HALF), cols], preferred_element_type=F32)
            hidden[:, cols] = (gate / (1.0 + jnp.exp(-gate)) * up).astype(BF16)
        for half in range(2):
            for n in range(2):
                at = pl.multiple_of(other_at + half * 512 + n * 256, 256)
                psend[r, half, :, n * 256 : n * 256 + 256] = jnp.dot(
                    hidden[...], wd[:, pl.ds(at, 256)], preferred_element_type=F32
                ).astype(BF16)
            pass_partial(r, half).start()
        for half in range(2):
            for n in range(2):
                at = pl.multiple_of(mine_at + half * 512 + n * 256, 256)
                pown[r, half, :, n * 256 : n * 256 + 256] = jnp.dot(
                    hidden[...], wd[:, pl.ds(at, 256)], preferred_element_type=F32
                ).astype(BF16)
        return carry

    lax.fori_loop(0, 4, ffn, 0)
    finish(3)

    sums[...] = jnp.zeros_like(sums)

    def combine(r, s):
        lo, width = SLICES[s]
        part = ret.at[pl.ds(r * 16, 15), :, pl.ds(lo, width)]
        remote(part, part, r_send, r_recv.at[r, s], partner).wait_recv()
        for c in range(4):
            rows = ret[pl.ds(r * 16 + c * 4, 4), :, lo : lo + width].reshape(4 * PICK, width)
            rows = jnp.concatenate([rows, jnp.zeros((128 - 4 * PICK, width), BF16)], axis=0)
            sums[c, :, lo : lo + width] += jnp.dot(
                pick[(s * 4 + r) * 4 + c], rows, preferred_element_type=F32
            )

    def combine_all(r, carry):
        for s in range(3):
            combine(r, s)
        return carry

    lax.fori_loop(0, 3, combine_all, 0)
    for s, (lo, width) in enumerate(SLICES):
        combine(3, s)
        cols = pl.ds(lo, width)
        for c in (2, 1, 3):
            rsend[c - 1, :, lo : lo + width] = sums[c, :, lo : lo + width].astype(BF16)
            remote(
                rsend.at[c - 1, :, cols], rrecv.at[c - 1, :, cols], q_send, q_recv.at[s],
                (peer(*offset_of(s, 0, 0, -c)), tp),
            ).start()
    for s, (lo, width) in enumerate(SLICES):
        part = rrecv.at[:, :, pl.ds(lo, width)]
        remote(part, part, q_send, q_recv.at[s], partner).wait_recv()
        total = sums[0, :, lo : lo + width]
        for c in range(3):
            total += rrecv[c, :, lo : lo + width].astype(F32)
        out[:, lo : lo + width] = total.astype(BF16)

    remote(passed.at[:, :, 0:3], passed.at[:, :, 1:4], i_send, i_recv, partner).wait_send()
    remote(irecv.at[:, 0:3], irecv.at[:, 1:4], j_send, j_recv, partner).wait_send()
    remote(gathered.at[0:3], gathered.at[1:4], g_send, g_recv, partner).wait_send()
    remote(dsend.at[0:60], dsend.at[0:60], d_send, d_recv.at[0], partner).wait_send()
    remote(own, other, f_send, f_recv.at[0], partner).wait_send()
    remote(psend, precv, p_send, p_recv.at[0, 0], partner).wait_send()
    remote(wt.at[0:60], ret.at[0:60], r_send, r_recv.at[0, 0], partner).wait_send()
    remote(rsend, rrecv, q_send, q_recv.at[0], partner).wait_send()


def on_device(tokens, chosen, gate_score, gate_weight, up_weight, down_weight):
    vmem = pl.BlockSpec(memory_space=pltpu.VMEM)
    hbm = pl.BlockSpec(memory_space=pl.ANY)
    dma = pltpu.SemaphoreType.DMA
    blocks = pltpu.VMEM((64, PICK, HALF), BF16)
    partial = pltpu.VMEM((4, 2, ROWS, 512), BF16)
    tiles = pltpu.VMEM((3, 4, 4, 8, 128), BF16)
    return pl.pallas_call(
        kernel,
        out_shape=jax.ShapeDtypeStruct((TOK, HALF), BF16),
        in_specs=[vmem, vmem, vmem, hbm, hbm, hbm],
        out_specs=vmem,
        scratch_shapes=[
            pltpu.VMEM((2048, 1024), BF16), pltpu.VMEM((2048, 1024), BF16), pltpu.VMEM((1024, 2048), BF16),
            pltpu.VMEM((4, TOK, HALF), BF16),
            tiles, tiles, tiles,
            pltpu.VMEM((48, TOK, 128), BF16),
            blocks, blocks, blocks,
            pltpu.VMEM((ROWS, 1024), F32), pltpu.VMEM((ROWS, 1024), F32), pltpu.VMEM((ROWS, 1024), BF16),
            partial, partial, partial,
            blocks, blocks,
            pltpu.VMEM((4, TOK, HALF), F32),
            pltpu.VMEM((3, TOK, HALF), BF16), pltpu.VMEM((3, TOK, HALF), BF16),
            pltpu.VMEM((64 * PICK, 128), F32),
            dma((3,)), dma, dma, dma, dma, dma, dma, dma, dma((4,)), dma, dma((4,)), dma, dma((4, 2)),
            dma, dma((4, 3)), dma, dma((3,)),
        ],
        compiler_params=pltpu.CompilerParams(
            collective_id=0, has_side_effects=True, vmem_limit_bytes=63 << 20
        ),
        cost_estimate=pl.CostEstimate(flops=20_000_000_000, bytes_accessed=14_000_000, transcendentals=1_600_000),
    )(tokens, chosen, gate_score, gate_weight[0], up_weight[0], down_weight[0])


def solution(mesh):
    in_specs = (
        P("ep", "tp"),
        P("ep", None),
        P("ep", None),
        P("ep", None, "tp"),
        P("ep", None, "tp"),
        P("ep", "tp", None),
    )
    out_specs = P("ep", "tp")
    return jax.shard_map(
        on_device, mesh=mesh, in_specs=in_specs, out_specs=out_specs, check_vma=False
    )
```

time: 87.8 us -> 77.7 us (0.88)
  Pallas kernels: 82.9 us -> 75.8 us
  other arithmetic: 1.43 us -> 0 us
  local copies, waits for them, and re-layouts: 3.16 us -> 1.77 us
    pallas_call x1, Pallas kernels: 82.9 us -> 75.8 us  [on_device(): pl.pallas_call(kernel, out_shape=jax.ShapeDtypeStruct((TOK, HALF), BF16),...]
    unnamed x2 -> x0, other arithmetic: 1.43 us -> none
    pad x2 -> x0, local copies, waits for them, and re-layouts: 1.23 us -> none  [the longest x1 0.62 us: on_device(): chosen = jnp.pad(chosen.reshape(64, PICK), ((0, 0), (0, 128 - PICK)))]
where the time goes in v2:
time: 77.7 us; the launch traced here: 77.6 us
  Pallas kernels  75.8 us (98%)
  local copies, waits for them, and re-layouts  1.77 us (2%)
    pallas_call x1, Pallas kernels, on_device(): pl.pallas_call(kernel, out_shape=jax.ShapeDtypeStruct((TOK, HALF), BF16),...  75.8 us
    unnamed x1, local copies, waits for them, and re-layouts  1.77 us

profile of v2, /device:TPU:1, one launch (start us, length us, event | category | flops | bytes accessed | tf_op | source)
XLA Modules:
  0.0 77.6 jit_solution(7560683420689164000)
XLA Ops:
  0.0 75.8 %shard_map.64 = bf16[192,1024]{1,0:T(8,128)(2,1)} custom-call(bf16[192,1024]{1,0:T(8,128)(2,1)} %tokens.1, s32[1,1536]{1,0:T(1,128)} %chosen.1, f32[1,1536]{1,0:T(1,128)} %score.1, bf16[2048,1024]{1,0:T(8,128)(2,1)} %bitcast.3, bf16[2048,1024]{1,0:T(8,128)(2,1)} %bitcast.4, bf16[1024,2048]{1,0:T(8,128)(2,1)} %bitcast.5), custom_call_target="tpu_custom_call" | custom-call | flops 20000000000 | bytes 14000000 | tf_op jit(solution)/shard_map/pallas_call | solution.py:310
  75.8 1.8 %copy.8 = bf16[192,1024]{1,0:T(8,128)(2,1)} copy(bf16[192,1024]{1,0:T(8,128)(2,1)} %shard_map.64) | data formatting | bytes 786432

commit v3 on v2

--- a/solution.py
+++ b/solution.py
@@ -11,8 +11,8 @@
 TOK = 192
 PICK = 24
 HALF = 1024
-ROWS = 16 * PICK
 CAP = 64 * PICK
+PART = 8 * PICK
 SLICES = ((0, 384), (384, 384), (768, 256))
 
 
@@ -51,9 +51,14 @@
 
     partner = (ep, 1 - tp)
 
+    def half_of(s, a, b, c):
+        _, du, dv = offset_of(s, a, b, c)
+        return (du // 2 + dv // 2) % 2
+
     def block_of(s, a, b, c):
-        dz, du, dv = offset_of(s, a, b, c)
-        return du * u_step + dv * v_step
+        _, du, dv = offset_of(s, a, b, c)
+        on_0, on_1 = du * 2 + dv % 2, dv * 2 + du % 2
+        return half_of(s, a, b, c) * 8 + on_0 + tp * (on_1 - on_0)
 
     weights = [
         pltpu.make_async_copy(src, dst, w_sem.at[i])
@@ -123,7 +128,8 @@
     gather(2, pl.ds(0, TOK))
 
     row = lax.broadcasted_iota(jnp.int32, (64, CAP), 0)
-    oy, ox = (row >> 2) & 3, row & 3
+    oy = (row >> 1) & 3
+    ox = 2 * (((oy >> 1) + (row >> 3)) & 1) + (row & 1)
     oz = ((row >> 4) - oy - ox) & 3
     src = ((z - oz) & 3) * 16 + ((y - oy) & 3) * 4 + ((x - ox) & 3)
     left = jnp.where(jnp.broadcast_to(home, (64, CAP)) == src, jnp.broadcast_to(score[...], (64, CAP)), 0.0)
@@ -158,53 +164,69 @@
                 blk = r * 16 + block_of(s, a, b, c)
                 if a == 0 and b == 0:
                     own[blk, :, lo : lo + width] = rows[0:PICK]
-                    continue
-                dsend[blk, :, lo : lo + width] = rows[a * PICK : (a + 1) * PICK]
-                remote(
-                    dsend.at[blk, :, cols], own.at[blk, :, cols], d_send, d_recv.at[r],
-                    (peer(*offset_of(s, a, b, 0)), tp),
-                ).start()
-
-    dispatch(0, 0)
-    dispatch(1, 0)
+                else:
+                    dsend[blk, :, lo : lo + width] = rows[a * PICK : (a + 1) * PICK]
+
+    def send_out(r, directions):
+        for half in range(2):
+            for c in directions:
+                for a in range(4):
+                    for s, (lo, width) in enumerate(SLICES):
+                        b = (r - c - a) % 4
+                        if (a == 0 and b == 0) or half_of(s, a, b, c) != half:
+                            continue
+                        blk, cols = r * 16 + block_of(s, a, b, c), pl.ds(lo, width)
+                        remote(
+                            dsend.at[blk, :, cols], own.at[blk, :, cols], d_send, d_recv.at[2 * r + half, s],
+                            (peer(*offset_of(s, a, b, 0)), tp),
+                        ).start()
+
+    for r in range(2):
+        dispatch(r, 0)
+        send_out(r, (0,))
     remote(gathered.at[0:3], gathered.at[1:4], g_send, g_recv, partner).wait_recv()
     for r in range(4):
-        for c in (0, 1, 3, 2):
-            if c or r > 1:
-                dispatch(r, c)
-
-    def forward(r):
-        chunk = pl.ds(r * 16, 16)
-        return remote(own.at[chunk], other.at[chunk], f_send, f_recv.at[r], partner)
-
-    def pass_partial(r, half):
-        return remote(psend.at[r, half], precv.at[r, half], p_send, p_recv.at[r, half], partner)
-
-    def arrived(r):
-        part = pl.ds(r * 16, 15)
-        remote(own.at[part], own.at[part], d_send, d_recv.at[r], partner).wait_recv()
-
-    def finish(r):
-        back = [lax.rem(r + 4 - k, 4) for k in range(4)]
-        first = pl.multiple_of(r * ROWS, ROWS)
-        factor = jnp.concatenate([scale[pl.ds(first, ROWS), :]] * 4, axis=1)
-        for half in range(2):
-            pass_partial(r, half).wait_recv()
-            summed = pown[r, half].astype(F32) + precv[r, half].astype(F32)
-            wt[pl.ds(r * 16, 16), :, half * 512 : half * 512 + 512] = (
-                (summed * factor).astype(BF16).reshape(16, PICK, 512)
-            )
-            for s, (lo, width) in enumerate(SLICES):
-                if (lo + width > 512) != (half == 1):
-                    continue
-                cols = pl.ds(lo, width)
-                ret[r * 20, :, lo : lo + width] = wt[r * 16 + block_of(s, 0, 0, r), :, lo : lo + width]
-                for j in range(1, 16):
-                    a, b = j // 4, j % 4
-                    c = back[(a + b) % 4]
+        rest = (1, 3, 2) if r < 2 else (0, 1, 3, 2)
+        for c in rest:
+            dispatch(r, c)
+        send_out(r, rest)
+
+    def forward(k):
+        part = pl.ds(k * 8, 8)
+        return remote(own.at[part], other.at[part], f_send, f_recv.at[k], partner)
+
+    def pass_partial(k):
+        return remote(psend.at[k], precv.at[k], p_send, p_recv.at[k], partner)
+
+    def arrived(k):
+        r, half = k // 2, k % 2
+        for s, (lo, width) in enumerate(SLICES):
+            count = 8 - (half_of(s, 0, 0, r) == half)
+            part = own.at[pl.ds(k * 8, count), :, pl.ds(lo, width)]
+            remote(part, part, d_send, d_recv.at[k, s], partner).wait_recv()
+
+    def finish(k):
+        r, half = k // 2, k % 2
+        pass_partial(k).wait_recv()
+        factor = jnp.concatenate([scale[k * PART : (k + 1) * PART, :]] * 4, axis=1)
+        for n in range(2):
+            cols = slice(n * 512, n * 512 + 512)
+            summed = pown[k, :, cols].astype(F32) + precv[k, :, cols].astype(F32)
+            wt[k * 8 : k * 8 + 8, :, cols] = (summed * factor).astype(BF16).reshape(8, PICK, 512)
+        for s, (lo, width) in enumerate(SLICES):
+            cols = pl.ds(lo, width)
+            for a in range(4):
+                for b in range(4):
+                    c = (r - a - b) % 4
+                    if half_of(s, a, b, c) != half:
+                        continue
+                    blk, place = r * 16 + block_of(s, a, b, c), r * 16 + c * 4 + a
+                    if a == 0 and b == 0:
+                        ret[place, :, lo : lo + width] = wt[blk, :, lo : lo + width]
+                        continue
                     remote(
-                        wt.at[r * 16 + block_of(s, a, b, c), :, cols], ret.at[r * 16 + c * 4 + a, :, cols],
-                        r_send, r_recv.at[r, s], (peer(*offset_of(s, -a, -b, 0)), tp),
+                        wt.at[blk, :, cols], ret.at[place, :, cols], r_send, r_recv.at[r, s],
+                        (peer(*offset_of(s, -a, -b, 0)), tp),
                     ).start()
 
     for copy in weights:
@@ -212,47 +234,46 @@
     mine_at = pl.multiple_of(tp * HALF, HALF)
     other_at = pl.multiple_of((1 - tp) * HALF, HALF)
 
-    def ffn(r, carry):
-        arrived(r)
-        forward(r).start()
-        x_own = own[pl.ds(r * 16, 16)].reshape(ROWS, HALF)
-        for n in range(4):
-            cols = slice(n * 256, (n + 1) * 256)
-            gate_acc[:, cols] = jnp.dot(x_own, wg[pl.ds(mine_at, HALF), cols], preferred_element_type=F32)
-
-        @pl.when(r > 0)
-        def _():
-            finish(r - 1)
-
-        for n in range(4):
-            cols = slice(n * 256, (n + 1) * 256)
-            up_acc[:, cols] = jnp.dot(x_own, wu[pl.ds(mine_at, HALF), cols], preferred_element_type=F32)
-        forward(r).wait_recv()
-        x_other = other[pl.ds(r * 16, 16)].reshape(ROWS, HALF)
-        for n in range(4):
-            cols = slice(n * 256, (n + 1) * 256)
-            gate = gate_acc[:, cols] + jnp.dot(
-                x_other, wg[pl.ds(other_at, HALF), cols], preferred_element_type=F32
-            )
-            up = up_acc[:, cols] + jnp.dot(x_other, wu[pl.ds(other_at, HALF), cols], preferred_element_type=F32)
+    tiles_of = [slice(n * 256, (n + 1) * 256) for n in range(4)]
+
+    def up_own(k):
+        rows = own[k * 8 : k * 8 + 8].reshape(PART, HALF)
+        for cols in tiles_of:
+            gate_acc[:, cols] = jnp.dot(rows, wg[pl.ds(mine_at, HALF), cols], preferred_element_type=F32)
+            up_acc[:, cols] = jnp.dot(rows, wu[pl.ds(mine_at, HALF), cols], preferred_element_type=F32)
+
+    def up_other(k):
+        rows = other[k * 8 : k * 8 + 8].reshape(PART, HALF)
+        for cols in tiles_of:
+            gate = gate_acc[:, cols] + jnp.dot(rows, wg[pl.ds(other_at, HALF), cols], preferred_element_type=F32)
+            up = up_acc[:, cols] + jnp.dot(rows, wu[pl.ds(other_at, HALF), cols], preferred_element_type=F32)
             hidden[:, cols] = (gate / (1.0 + jnp.exp(-gate)) * up).astype(BF16)
-        for half in range(2):
-            for n in range(2):
-                at = pl.multiple_of(other_at + half * 512 + n * 256, 256)
-                psend[r, half, :, n * 256 : n * 256 + 256] = jnp.dot(
-                    hidden[...], wd[:, pl.ds(at, 256)], preferred_element_type=F32
-                ).astype(BF16)
-            pass_partial(r, half).start()
-        for half in range(2):
-            for n in range(2):
-                at = pl.multiple_of(mine_at + half * 512 + n * 256, 256)
-                pown[r, half, :, n * 256 : n * 256 + 256] = jnp.dot(
-                    hidden[...], wd[:, pl.ds(at, 256)], preferred_element_type=F32
-                ).astype(BF16)
-        return carry
-
-    lax.fori_loop(0, 4, ffn, 0)
-    finish(3)
+
+    def down(k):
+        for n, cols in enumerate(tiles_of):
+            at = pl.multiple_of(other_at + n * 256, 256)
+            psend[k, :, cols] = jnp.dot(
+                hidden[...], wd[:, pl.ds(at, 256)], preferred_element_type=F32
+            ).astype(BF16)
+        pass_partial(k).start()
+        for n, cols in enumerate(tiles_of):
+            at = pl.multiple_of(mine_at + n * 256, 256)
+            pown[k, :, cols] = jnp.dot(
+                hidden[...], wd[:, pl.ds(at, 256)], preferred_element_type=F32
+            ).astype(BF16)
+
+    for k in range(8):
+        arrived(k)
+        forward(k).start()
+        up_own(k)
+        if k:
+            down(k - 1)
+        forward(k).wait_recv()
+        up_other(k)
+        if k:
+            finish(k - 1)
+    down(7)
+    finish(7)
 
     sums[...] = jnp.zeros_like(sums)
 
@@ -293,9 +314,9 @@
     remote(passed.at[:, :, 0:3], passed.at[:, :, 1:4], i_send, i_recv, partner).wait_send()
     remote(irecv.at[:, 0:3], irecv.at[:, 1:4], j_send, j_recv, partner).wait_send()
     remote(gathered.at[0:3], gathered.at[1:4], g_send, g_recv, partner).wait_send()
-    remote(dsend.at[0:60], dsend.at[0:60], d_send, d_recv.at[0], partner).wait_send()
+    remote(dsend.at[0:60], dsend.at[0:60], d_send, d_recv.at[0, 0], partner).wait_send()
     remote(own, other, f_send, f_recv.at[0], partner).wait_send()
-    remote(psend, precv, p_send, p_recv.at[0, 0], partner).wait_send()
+    remote(psend, precv, p_send, p_recv.at[0], partner).wait_send()
     remote(wt.at[0:60], ret.at[0:60], r_send, r_recv.at[0, 0], partner).wait_send()
     remote(rsend, rrecv, q_send, q_recv.at[0], partner).wait_send()
 
@@ -305,7 +326,7 @@
     hbm = pl.BlockSpec(memory_space=pl.ANY)
     dma = pltpu.SemaphoreType.DMA
     blocks = pltpu.VMEM((64, PICK, HALF), BF16)
-    partial = pltpu.VMEM((4, 2, ROWS, 512), BF16)
+    partial = pltpu.VMEM((8, PART, HALF), BF16)
     tiles = pltpu.VMEM((3, 4, 4, 8, 128), BF16)
     return pl.pallas_call(
         kernel,
@@ -318,13 +339,13 @@
             tiles, tiles, tiles,
             pltpu.VMEM((48, TOK, 128), BF16),
             blocks, blocks, blocks,
-            pltpu.VMEM((ROWS, 1024), F32), pltpu.VMEM((ROWS, 1024), F32), pltpu.VMEM((ROWS, 1024), BF16),
+            pltpu.VMEM((PART, 1024), F32), pltpu.VMEM((PART, 1024), F32), pltpu.VMEM((PART, 1024), BF16),
             partial, partial, partial,
             blocks, blocks,
             pltpu.VMEM((4, TOK, HALF), F32),
             pltpu.VMEM((3, TOK, HALF), BF16), pltpu.VMEM((3, TOK, HALF), BF16),
             pltpu.VMEM((64 * PICK, 128), F32),
-            dma((3,)), dma, dma, dma, dma, dma, dma, dma, dma((4,)), dma, dma((4,)), dma, dma((4, 2)),
+            dma((3,)), dma, dma, dma, dma, dma, dma, dma, dma((8, 3)), dma, dma((8,)), dma, dma((8,)),
             dma, dma((4, 3)), dma, dma((3,)),
         ],
         compiler_params=pltpu.CompilerParams(

time: 77.7 us -> 76.9 us (0.990)
  Pallas kernels: 75.8 us -> 75 us
    pallas_call x1, Pallas kernels: 75.8 us -> 75 us  [on_device(): pl.pallas_call(kernel, out_shape=jax.ShapeDtypeStruct((TOK, HALF), BF16),...]
where the time goes in v3:
time: 76.9 us; the launch traced here: 76.8 us
  Pallas kernels  75 us (98%)
  local copies, waits for them, and re-layouts  1.77 us (2%)
    pallas_call x1, Pallas kernels, on_device(): pl.pallas_call(kernel, out_shape=jax.ShapeDtypeStruct((TOK, HALF), BF16),...  75 us
    unnamed x1, local copies, waits for them, and re-layouts  1.77 us

profile of v3, /device:TPU:1, one launch (start us, length us, event | category | flops | bytes accessed | tf_op | source)
XLA Modules:
  0.0 76.8 jit_solution(13912300732462050648)
XLA Ops:
  0.0 75.0 %shard_map.64 = bf16[192,1024]{1,0:T(8,128)(2,1)} custom-call(bf16[192,1024]{1,0:T(8,128)(2,1)} %tokens.1, s32[1,1536]{1,0:T(1,128)} %chosen.1, f32[1,1536]{1,0:T(1,128)} %score.1, bf16[2048,1024]{1,0:T(8,128)(2,1)} %bitcast.3, bf16[2048,1024]{1,0:T(8,128)(2,1)} %bitcast.4, bf16[1024,2048]{1,0:T(8,128)(2,1)} %bitcast.5), custom_call_target="tpu_custom_call" | custom-call | flops 20000000000 | bytes 14000000 | tf_op jit(solution)/shard_map/pallas_call | solution.py:331
  75.0 1.8 %copy.8 = bf16[192,1024]{1,0:T(8,128)(2,1)} copy(bf16[192,1024]{1,0:T(8,128)(2,1)} %shard_map.64) | data formatting | bytes 786432

commit v4 on v3

--- a/solution.py
+++ b/solution.py
@@ -81,21 +81,25 @@
     place = lax.broadcasted_iota(jnp.int32, (CAP, 128), 0)
     place -= PICK * ((place.astype(F32) + 0.5) * (1.0 / PICK)).astype(jnp.int32)
     place = lax.broadcasted_iota(jnp.int32, (CAP, 128), 1) - place
-    row = lax.broadcasted_iota(jnp.int32, (32, CAP), 0)
-    ib, ic = row >> 3, row & 7
-    homes = jnp.broadcast_to(home, (32, CAP))
-    locals_ = jnp.broadcast_to(local, (32, CAP))
-    for a in range(4):
-        spread = jnp.where(place == a * PICK, 1.0, 0.0).astype(BF16)
-        for s in range(3):
-            oz, ou, ov = offset_of(s, a, ib, ic)
-            src = ((z - oz) & 3) * 16 + ((u - ou) & 3) * u_step + ((v - ov) & 3) * v_step
-            src = jnp.where(ic < 4, src, -1)
-            take = jnp.where(homes == src, locals_, 0.0).astype(BF16)
-            rows = jnp.dot(take, spread, preferred_element_type=F32).astype(BF16)
-            isend[s, a] = rows.reshape(4, 8, 128)
+    row = lax.broadcasted_iota(jnp.int32, (128, 128), 0)
+    ia, ib, ic = row >> 5, (row >> 3) & 3, row & 7
+    homes = jnp.broadcast_to(home, (128, CAP))
+    locals_ = jnp.broadcast_to(local, (128, CAP))
+    takes = []
+    for s in range(3):
+        oz, ou, ov = offset_of(s, ia, ib, ic)
+        src = ((z - oz) & 3) * 16 + ((u - ou) & 3) * u_step + ((v - ov) & 3) * v_step
+        src = jnp.concatenate([jnp.where(ic < 4, src, -1)] * (CAP // 128), axis=1)
+        takes.append(jnp.where(homes == src, locals_, 0.0).astype(BF16))
+    spread = jnp.where(place == 0, 1.0, 0.0).astype(BF16)
+    rows = jnp.dot(jnp.concatenate(takes, axis=0), spread, preferred_element_type=F32)
+    for s in range(3):
+        for a in range(4):
+            tile = rows[128 * s + 32 * a : 128 * s + 32 * a + 32]
+            tile = (tile if a == 0 else pltpu.roll(tile, a * PICK, 1)).astype(BF16).reshape(4, 8, 128)
+            isend[s, a] = tile
             if a == 0:
-                passed[s, :, 0] = rows.reshape(4, 8, 128)
+                passed[s, :, 0] = tile
     gathered[0] = tokens[...]
 
     pl.semaphore_wait(barrier, 10)
@@ -114,8 +118,8 @@
                 (peer(*offset_of(s, 0, 0, c)), tp),
             ).start()
 
-    gather(1, pl.ds(0, 128))
-    gather(3, pl.ds(0, 128))
+    gather(1, pl.ds(0, TOK))
+    gather(3, pl.ds(0, TOK))
     remote(passed.at[:, :, 0:3], passed.at[:, :, 1:4], i_send, i_recv, partner).wait_recv()
     for s in range(3):
         for b in (2, 1, 3):
@@ -123,17 +127,15 @@
                 passed.at[s, b], irecv.at[s, b], j_send, j_recv, (peer(*offset_of(s, 0, -b, 0)), tp)
             ).start()
         irecv[s, 0] = passed[s, 0]
-    gather(1, pl.ds(128, 64))
-    gather(3, pl.ds(128, 64))
     gather(2, pl.ds(0, TOK))
 
-    row = lax.broadcasted_iota(jnp.int32, (64, CAP), 0)
+    row = lax.broadcasted_iota(jnp.int32, (64, 128), 0)
     oy = (row >> 1) & 3
     ox = 2 * (((oy >> 1) + (row >> 3)) & 1) + (row & 1)
     oz = ((row >> 4) - oy - ox) & 3
     src = ((z - oz) & 3) * 16 + ((y - oy) & 3) * 4 + ((x - ox) & 3)
+    src = jnp.concatenate([src] * (CAP // 128), axis=1)
     left = jnp.where(jnp.broadcast_to(home, (64, CAP)) == src, jnp.broadcast_to(score[...], (64, CAP)), 0.0)
-    spread = jnp.where(place == 0, 1.0, 0.0).astype(BF16)
     ordered = jnp.zeros((64, 128), F32)
     for _ in range(3):
         term = left.astype(BF16)
@@ -213,21 +215,30 @@
             cols = slice(n * 512, n * 512 + 512)
             summed = pown[k, :, cols].astype(F32) + precv[k, :, cols].astype(F32)
             wt[k * 8 : k * 8 + 8, :, cols] = (summed * factor).astype(BF16).reshape(8, PICK, 512)
-        for s, (lo, width) in enumerate(SLICES):
-            cols = pl.ds(lo, width)
-            for a in range(4):
-                for b in range(4):
-                    c = (r - a - b) % 4
-                    if half_of(s, a, b, c) != half:
-                        continue
-                    blk, place = r * 16 + block_of(s, a, b, c), r * 16 + c * 4 + a
-                    if a == 0 and b == 0:
-                        ret[place, :, lo : lo + width] = wt[blk, :, lo : lo + width]
-                        continue
-                    remote(
-                        wt.at[blk, :, cols], ret.at[place, :, cols], r_send, r_recv.at[r, s],
-                        (peer(*offset_of(s, -a, -b, 0)), tp),
-                    ).start()
+        for n in range(3):
+            if n == 0 or k != 6:
+                send_back(k, n)
+            if n == 0 and k == 7:
+                send_back(6, 1)
+                send_back(6, 2)
+
+    def send_back(k, s):
+        r, half = k // 2, k % 2
+        lo, width = SLICES[s]
+        cols = pl.ds(lo, width)
+        for a in range(4):
+            for b in range(4):
+                c = (r - a - b) % 4
+                if half_of(s, a, b, c) != half:
+                    continue
+                blk, place = r * 16 + block_of(s, a, b, c), r * 16 + c * 4 + a
+                if a == 0 and b == 0:
+                    ret[place, :, lo : lo + width] = wt[blk, :, lo : lo + width]
+                    continue
+                remote(
+                    wt.at[blk, :, cols], ret.at[place, :, cols], r_send, r_recv.at[r, s],
+                    (peer(*offset_of(s, -a, -b, 0)), tp),
+                ).start()
 
     for copy in weights:
         copy.wait()

time: 76.9 us -> 76.8 us (level)
  no operation moved by 1% of the time
where the time goes in v4:
time: 76.8 us; the launch traced here: 76.6 us
  Pallas kernels  74.9 us (98%)
  local copies, waits for them, and re-layouts  1.77 us (2%)
    pallas_call x1, Pallas kernels, on_device(): pl.pallas_call(kernel, out_shape=jax.ShapeDtypeStruct((TOK, HALF), BF16),...  74.9 us
    unnamed x1, local copies, waits for them, and re-layouts  1.77 us

profile of v4, /device:TPU:1, one launch (start us, length us, event | category | flops | bytes accessed | tf_op | source)
XLA Modules:
  0.0 76.6 jit_solution(12064811581037795716)
XLA Ops:
  0.0 74.9 %shard_map.64 = bf16[192,1024]{1,0:T(8,128)(2,1)} custom-call(bf16[192,1024]{1,0:T(8,128)(2,1)} %tokens.1, s32[1,1536]{1,0:T(1,128)} %chosen.1, f32[1,1536]{1,0:T(1,128)} %score.1, bf16[2048,1024]{1,0:T(8,128)(2,1)} %bitcast.3, bf16[2048,1024]{1,0:T(8,128)(2,1)} %bitcast.4, bf16[1024,2048]{1,0:T(8,128)(2,1)} %bitcast.5), custom_call_target="tpu_custom_call" | custom-call | flops 20000000000 | bytes 14000000 | tf_op jit(solution)/shard_map/pallas_call | solution.py:342
  74.9 1.8 %copy.8 = bf16[192,1024]{1,0:T(8,128)(2,1)} copy(bf16[192,1024]{1,0:T(8,128)(2,1)} %shard_map.64) | data formatting | bytes 786432
